TPU v7x, 32 devices: a whole 2x2x4 slice. The times are simulated.
32 devices in a mesh: kv: 8 (over z, x), tp: 4 (over y, core).
Axes of the slice: x: 2, y: 2, z: 4, core: 2. Of those that a mesh axis runs over, the one named last changes fastest.
Arguments:
- hidden: bfloat16 [128, 4, 2048], P(None, None, 'kv'), may hold values from -18 to 18
- norm_gain: float32 [2048], replicated, may hold values from 0.1 to 1.9
- w_query: bfloat16 [2048, 1024], P(None, 'tp'), may hold values from -0.125 to 0.125
- w_forget: bfloat16 [2048, 1024], P(None, 'tp'), may hold values from -0.125 to 0.125
- w_input: bfloat16 [2048, 1024], P(None, 'tp'), may hold values from -0.125 to 0.125
- w_outgate: bfloat16 [2048, 1024], P(None, 'tp'), may hold values from -0.125 to 0.125
- w_out: bfloat16 [1024, 2048], replicated, may hold values from -0.1875 to 0.1875
- floor: float32 [1024], P('tp'), may hold values from 0 to 0.95
- head_gain: float32 [128], replicated, may hold values from 0.1 to 1.9
- base_state: float32 [128, 8, 128, 128], P('kv', 'tp'), may hold values from -4 to 4
- prev_forget: bfloat16 [128, 4, 1024], P('kv', None, 'tp'), may hold values from -6 to 6
- prev_input: bfloat16 [128, 4, 1024], P('kv', None, 'tp'), may hold values from -6 to 6
- accepted: int32 [128], P('kv'), may hold values from 0 to 4
Outputs:
- mixed: bfloat16 [128, 4, 2048], P(None, None, 'kv')
- taken_state: float32 [128, 8, 128, 128], P('kv', 'tp')
All inputs are finite; a program needn't handle non-finite values.
Results may differ from a plain program's by a relative error of at most 0.014.
Values may be sent and summed in bfloat16 or wider, within the bound.
A program may use at most 64 MiB of HBM per device.

v0:
```python
import jax
import jax.numpy as jnp
from jax import lax
from jax.sharding import PartitionSpec as P

D = 2048
HEAD_DIM = 128
PROPS = 4


def shards(
    hidden,
    norm_gain,
    w_query,
    w_forget,
    w_input,
    w_outgate,
    w_out,
    floor,
    head_gain,
    base_state,
    prev_forget,
    prev_input,
    accepted,
):
    arrived = lax.all_to_all(hidden, "kv", split_axis=0, concat_axis=2, tiled=True)
    whole_vals = arrived.astype(jnp.float32)
    row_sums = jnp.sum(whole_vals * whole_vals, axis=2)
    normed = (whole_vals * lax.rsqrt(row_sums / D + 1e-06)[..., None] * norm_gain).astype(
        jnp.bfloat16
    )
    query_pre = jnp.dot(normed, w_query, preferred_element_type=jnp.float32).astype(jnp.bfloat16)
    forget_pre = jnp.dot(normed, w_forget, preferred_element_type=jnp.float32).astype(jnp.bfloat16)
    input_pre = jnp.dot(normed, w_input, preferred_element_type=jnp.float32).astype(jnp.bfloat16)
    gate_pre = jnp.dot(normed, w_outgate, preferred_element_type=jnp.float32).astype(jnp.bfloat16)
    seq_local = normed.shape[0]
    head_local = w_query.shape[1] // HEAD_DIM
    shape = (seq_local, PROPS, head_local, HEAD_DIM)
    query = jax.nn.silu(query_pre.astype(jnp.float32)).reshape(shape)
    forget = (floor + (1.0 - floor) * jax.nn.sigmoid(forget_pre.astype(jnp.float32))).reshape(shape)
    value = input_pre.astype(jnp.float32).reshape(shape)
    prev_f = (floor + (1.0 - floor) * jax.nn.sigmoid(prev_forget.astype(jnp.float32))).reshape(
        shape
    )
    prev_v = prev_input.astype(jnp.float32).reshape(shape)
    state = base_state
    for step in range(PROPS):
        live = (step < accepted)[:, None, None, None]
        moved = (
            prev_f[:, step][..., None] * state
            + (1.0 - prev_f[:, step])[..., None] * prev_v[:, step][:, :, None, :]
        )
        state = jnp.where(live, moved, state)
    taken_state = state
    outputs = []
    for step in range(PROPS):
        state = (
            forget[:, step][..., None] * state
            + (1.0 - forget[:, step])[..., None] * value[:, step][:, :, None, :]
        )
        outputs.append(
            jnp.einsum("bhk,bhkv->bhv", query[:, step], state, precision=lax.Precision.HIGHEST)
        )
    result = jnp.stack(outputs, axis=1)
    scaled = (
        result * lax.rsqrt(jnp.mean(result * result, axis=-1, keepdims=True) + 1e-05) * head_gain
    )
    gated = scaled * jax.nn.silu(gate_pre.astype(jnp.float32)).reshape(shape)
    mixed_heads = gated.reshape(seq_local, PROPS, head_local * HEAD_DIM).astype(jnp.bfloat16)
    own_rows = mixed_heads.shape[2]
    w_rows = lax.dynamic_slice_in_dim(w_out, lax.axis_index("tp") * own_rows, own_rows, 0)
    partial_value = jnp.dot(mixed_heads, w_rows, preferred_element_type=jnp.float32)
    finished = lax.psum(partial_value, "tp").astype(jnp.bfloat16)
    mixed = lax.all_to_all(finished, "kv", split_axis=2, concat_axis=0, tiled=True)
    return (mixed, taken_state)


def solution(mesh):
    placed = (
        P(None, None, "kv"),
        P(),
        P(None, "tp"),
        P(None, "tp"),
        P(None, "tp"),
        P(None, "tp"),
        P(),
        P("tp"),
        P(),
        P("kv", "tp", None, None),
        P("kv", None, "tp"),
        P("kv", None, "tp"),
        P("kv"),
    )
    return jax.shard_map(
        shards,
        mesh=mesh,
        in_specs=placed,
        out_specs=(P(None, None, "kv"), P("kv", "tp", None, None)),
        check_vma=False,
    )
```

profile of v0, /device:TPU:0, one launch (start us, length us, event | category | flops | bytes accessed | tf_op | source)
XLA Modules:
  0.0 96.0 jit_solution(18002514994027775703)
XLA Ops:
  0.6 7.4 %all-to-all-start = ((bf16[128,4,256]{2,1,0:T(4,128)(2,1)}), bf16[128,4,256]{2,1,0:T(4,128)(2,1)S(1)}, u32[]{:S(2)}, u32[]{:S(2)}) async-start(bf16[128,4,256]{2,1,0:T(4,128)(2,1)} %param.13), calls=%async_computation | async-start | bytes 524288 | tf_op jit(solution)/shard_map/all_to_all | solution.py:26
  8.1 0.7 broadcast_subtract_fusion.8
  8.8 0.6 copy-done.3
  9.3 0.8 multiply_add_fusion.9
  10.2 1.2 %broadcast_bitcast_fusion = f32[256]{0:T(256)} fusion(f32[128]{0:T(128)} %param.21), kind=kLoop, calls=%fused_computation.82 | loop fusion | bytes 1536 | tf_op jit(solution)/shard_map/mul | solution.py:66
  11.5 1.3 %broadcast_compare_fusion.3 = (pred[16]{0:T(512)(128)(4,1)}, pred[16]{0:T(512)(128)(4,1)}, pred[16]{0:T(512)(128)(4,1)}, pred[16]{0:T(512)(128)(4,1)}) fusion(s32[16]{0:T(128)} %param.25), kind=kLoop, calls=%fused_computation.88 | loop fusion | flops 64 | bytes 128 | tf_op jit(solution)/shard_map/gt | solution.py:48
  12.7 0.8 reshape.130
  13.5 0.6 slice_bitcast_fusion.10
  14.1 7.1 %add_select_fusion = f32[16,2,128,128]{3,2,1,0:T(8,128)S(1)} fusion(f32[16,2,128,128]{3,2,1,0:T(8,128)} %param.22, f32[16,2,128]{2,1,0:T(2,128)} %get-tuple-element.29, f32[16,2,128]{2,1,0:T(2,128)S(1)} %get-tuple-element.25, f32[16,2,128]{2,1,0:T(2,128)} %get-tuple-element.27, f32[16,2,128]{2,1,0:T(2,128)S(1)} %get-tuple-element.24, ...), kind=kLoop, calls=%fused_computation.7 | loop fusion | flops 8388608 | bytes 4390976 | tf_op jit(solution)/shard_map/jit(_where)/select_n | solution.py:53
  21.3 0.2 multiply_reduce_fusion
  21.7 1.1 %copy.38 = f32[16,4,8,256]{3,2,0,1:T(8,128)} copy(f32[16,4,8,256]{3,1,0,2:T(4,128)S(1)} %bitcast.141) | data formatting | bytes 1048576 | tf_op jit(solution)/shard_map/convert_element_type | solution.py:27
  22.8 1.9 %reshape.128 = f32[16,4,2048]{2,0,1:T(8,128)} reshape(f32[16,4,8,256]{3,2,0,1:T(8,128)} %copy.38) | data formatting | bytes 1048576 | tf_op jit(solution)/shard_map/convert_element_type | solution.py:27
  24.8 1.2 %multiply_convert_fusion = bf16[16,4,2048]{2,0,1:T(8,128)(2,1)S(1)} fusion(f32[16,4,2048]{2,0,1:T(8,128)} %reshape.128, f32[2048]{0:T(1024)S(1)} %copy-done.5, f32[16,4]{0,1:T(4,128)S(1)} %add_rsqrt_fusion.1), kind=kLoop, calls=%fused_computation.43 | loop fusion | flops 393216 | bytes 794880 | tf_op jit(solution)/shard_map/convert_element_type | solution.py:29
  25.9 1.5 %fusion.14 = f32[16,4,256]{2,0,1:T(8,128)S(1)} fusion(bf16[16,4,2048]{2,0,1:T(8,128)(2,1)S(1)} %multiply_convert_fusion, bf16[2048,256]{1,0:T(8,128)(2,1)} %param.16, f32[256]{0:T(256)S(1)} %copy-done.4, f32[256]{0:T(256)S(1)} %copy-done.2), kind=kOutput, calls=%fused_computation.21 | convolution fusion | flops 67223552 | bytes 1378304 | tf_op jit(solution)/shard_map/dot_general | solution.py:33
  27.5 1.5 %fusion.7 = f32[16,4,256]{2,0,1:T(8,128)S(1)} fusion(bf16[16,4,2048]{2,0,1:T(8,128)(2,1)S(1)} %multiply_convert_fusion, bf16[2048,256]{1,0:T(8,128)(2,1)} %param.17), kind=kOutput, calls=%fused_computation.13 | convolution fusion | flops 67141632 | bytes 1376256 | tf_op jit(solution)/shard_map/dot_general | solution.py:34
  29.1 0.7 reshape.132
  29.7 2.2 %divide_multiply_fusion = f32[16,4,256]{2,0,1:T(8,128)} fusion(bf16[16,4,2048]{2,0,1:T(8,128)(2,1)S(1)} %multiply_convert_fusion, bf16[2048,256]{1,0:T(8,128)(2,1)} %param.15), kind=kOutput, calls=%fused_computation.53 | convolution fusion | flops 67207168 | bytes 1376256 | tf_op jit(solution)/shard_map/dot_general | solution.py:32
  31.9 0.9 reshape.121
  32.8 0.8 slice_bitcast_fusion.6
  33.6 2.8 %fusion.4 = f32[16,2,1,128]{3,2,1,0:T(1,128)S(1)} fusion(f32[16,2,128,1]{2,3,1,0:T(1,128)S(1)} %bitcast.146, f32[16,2,128,128]{3,2,1,0:T(8,128)S(1)} %add_select_fusion, f32[16,2,128]{2,1,0:T(2,128)S(1)} %get-tuple-element.14, f32[16,2,128]{2,1,0:T(2,128)S(1)} %get-tuple-element.10, f32[16,2,128]{2,1,0:T(2,128)S(1)} %get-tuple-element.37), kind=kOutput, calls=%fused_computation.8 | convolution fusion | flops 7864320 | bytes 2179072 | tf_op jit(solution)/shard_map/bhk,bhkv->bhv/dot_general | solution.py:62
  36.4 4.3 %fusion.35 = f32[16,2,1,128]{3,2,1,0:T(1,128)S(1)} fusion(f32[16,2,128,1]{2,3,1,0:T(1,128)S(1)} %bitcast.155, f32[16,2,128,128]{3,2,1,0:T(8,128)S(1)} %add_select_fusion, f32[16,2,128]{2,1,0:T(2,128)S(1)} %get-tuple-element.17, f32[16,2,128]{2,1,0:T(2,128)S(1)} %get-tuple-element.13, f32[16,2,128]{2,1,0:T(2,128)S(1)} %get-tuple-element.34, ...), kind=kOutput, calls=%fused_computation.45 | convolution fusion | flops 9437184 | bytes 2228224 | tf_op jit(solution)/shard_map/bhk,bhkv->bhv/dot_general | solution.py:62
  40.7 6.1 %fusion.5 = f32[16,2,1,128]{3,2,1,0:T(1,128)S(1)} fusion(f32[16,2,128,1]{2,3,1,0:T(1,128)S(1)} %bitcast.154, f32[16,2,128]{2,1,0:T(2,128)S(1)} %get-tuple-element.16, f32[16,2,128]{2,1,0:T(2,128)S(1)} %get-tuple-element.12, f32[16,2,128]{2,1,0:T(2,128)S(1)} %get-tuple-element.35, f32[16,2,128,128]{3,2,1,0:T(8,128)S(1)} %add_select_fusion, ...), kind=kOutput, calls=%fused_computation.9 | convolution fusion | flops 11010048 | bytes 2277376 | tf_op jit(solution)/shard_map/bhk,bhkv->bhv/dot_general | solution.py:62
  46.8 7.2 %fusion = f32[16,2,1,128]{3,2,1,0:T(1,128)S(1)} fusion(f32[16,2,128,1]{2,3,1,0:T(1,128)S(1)} %bitcast.153, f32[16,2,128]{2,1,0:T(2,128)S(1)} %get-tuple-element.15, f32[16,2,128]{2,1,0:T(2,128)S(1)} %get-tuple-element.11, f32[16,2,128]{2,1,0:T(2,128)S(1)} %get-tuple-element.36, f32[16,2,128]{2,1,0:T(2,128)S(1)} %get-tuple-element.16, ...), kind=kOutput, calls=%fused_computation | convolution fusion | flops 12582912 | bytes 2326528 | tf_op jit(solution)/shard_map/bhk,bhkv->bhv/dot_general | solution.py:62
  54.1 0.1 fusion.39
  54.2 0.1 mul.343
  54.4 2.0 %fusion.16 = f32[16,4,2048]{2,0,1:T(8,128)S(1)} fusion(bf16[1024,2048]{1,0:T(8,128)(2,1)} %param.19, s32[]{:T(128)S(6)} %select_n.20, f32[16,4,256]{2,0,1:T(8,128)S(1)} %mul.344, f32[16,1,256]{2,0,1:T(8,128)S(1)} %stack.28, f32[16,1,256]{2,0,1:T(8,128)S(1)} %stack.27, f32[16,1,256]{2,0,1:T(8,128)S(1)} %stack.26, f32[16,1,256]{2,0,1:T(8,128)S(1)} %stack.25, ...), kind=kOutput, calls=%fused_computation.24 | convolution fusion | flops 134430720 | bytes 3015684 | tf_op jit(solution)/shard_map/dot_general | solution.py:72
  56.5 16.6 %all-reduce.1 = bf16[16,4,2048]{2,0,1:T(8,128)(2,1)S(1)} all-reduce(f32[16,4,2048]{2,0,1:T(8,128)S(1)} %fusion.16), channel_id=1, replica_groups=mesh['kv'=8,'tp'=4] {'tp'}, use_global_device_ids=true, to_apply=%region_3.4 | all-reduce | flops 131072 | bytes 786432 | tf_op jit(solution)/shard_map/psum | solution.py:73
  73.1 1.4 %copy.45 = bf16[16,4,2048]{0,1,2:T(4,128)(2,1)S(1)} copy(bf16[16,4,2048]{2,0,1:T(8,128)(2,1)S(1)} %all-reduce.1) | data formatting | bytes 524288 | tf_op jit(solution)/shard_map/convert_element_type | solution.py:73
  74.5 2.2 %reshape.148 = bf16[8,2,8192]{2,1,0:T(2,128)(2,1)S(1)} reshape(bf16[2048,4,16]{2,1,0:T(4,128)(2,1)S(1)} %bitcast.139) | data formatting | bytes 524288
  76.7 14.9 %all_to_all.27 = bf16[8,2,8192]{2,1,0:T(2,128)(2,1)} all-to-all(bf16[8,2,8192]{2,1,0:T(2,128)(2,1)S(1)} %reshape.148), channel_id=1, replica_groups=mesh['kv'=8,'tp'=4] {'kv'}, dimensions={0} | all-to-all | bytes 524288 | tf_op jit(solution)/shard_map/all_to_all | solution.py:74
  91.5 2.4 %reshape.149 = bf16[2048,4,16]{2,1,0:T(4,128)(2,1)S(1)} reshape(bf16[8,2,8192]{2,1,0:T(2,128)(2,1)} %all_to_all.27) | data formatting | bytes 524288
  94.0 2.0 %copy.46 = bf16[8,16,4,256]{3,2,1,0:T(4,128)(2,1)} copy(bf16[8,16,4,256]{1,2,3,0:T(4,128)(2,1)S(1)} %bitcast.140) | data formatting | bytes 524288 | tf_op jit(solution)/shard_map/all_to_all | solution.py:74
  (30 shorter events, 0.5 us)
Async XLA Ops:
  0.6 53.8 %copy-start = (bf16[2048,256]{1,0:T(8,128)(2,1)S(1)}, bf16[2048,256]{1,0:T(8,128)(2,1)}, u32[]{:S(2)}) copy-start(bf16[2048,256]{1,0:T(8,128)(2,1)} %param.18) | copy-start | bytes 3145732
  0.6 20.7 %all-to-all-start = ((bf16[128,4,256]{2,1,0:T(4,128)(2,1)}), bf16[128,4,256]{2,1,0:T(4,128)(2,1)S(1)}, u32[]{:S(2)}, u32[]{:S(2)}) async-start(bf16[128,4,256]{2,1,0:T(4,128)(2,1)} %param.13), calls=%async_computation | async-start | bytes 524288 | tf_op jit(solution)/shard_map/all_to_all | solution.py:26
  8.8 0.6 copy-start.3
  21.3 25.5 %copy-start.1 = (f32[16,2,128,128]{3,2,1,0:T(8,128)}, f32[16,2,128,128]{3,2,1,0:T(8,128)S(1)}, u32[]{:S(2)}) copy-start(f32[16,2,128,128]{3,2,1,0:T(8,128)S(1)} %add_select_fusion) | copy-start | bytes 6291460
  21.3 3.5 %copy-start.5 = (f32[2048]{0:T(1024)S(1)}, f32[2048]{0:T(1024)}, u32[]{:S(2)}) copy-start(f32[2048]{0:T(1024)} %param.14) | copy-start | bytes 24580
  21.3 4.6 %copy-start.2 = (f32[256]{0:T(256)S(1)}, f32[256]{0:T(256)}, u32[]{:S(2)}) copy-start(f32[256]{0:T(256)} %param.20) | copy-start | bytes 3076
  21.3 4.6 %copy-start.4 = (f32[256]{0:T(256)S(1)}, f32[256]{0:T(256)}, u32[]{:S(2)}) copy-start(f32[256]{0:T(256)} %copy-done.3) | copy-start | bytes 3076
  46.8 7.7 %copy-start.6 = (f32[256]{0:T(256)S(1)}, f32[256]{0:T(256)}, u32[]{:S(2)}) copy-start(f32[256]{0:T(256)} %broadcast_bitcast_fusion) | copy-start | bytes 3076
where the time goes:
time: 96.9 us; the launch traced here: 96 us
  blocking collectives  31.5 us (33%)
  matrix products  27.6 us (28%)
  local copies, waits for them, and re-layouts  17 us (18%)
  other arithmetic  11.5 us (12%)
  starting transfers between devices  7.42 us (8%)
    dot_general x4, matrix products, shards(): jnp.einsum('bhk,bhkv->bhv', query[:, step], state, precision=lax.Precisio...  20.3 us
    psum x1, blocking collectives, shards(): finished = lax.psum(partial_value, 'tp').astype(jnp.bfloat16)  16.6 us
    all_to_all x1, blocking collectives, shards(): lax.all_to_all(finished, 'kv', split_axis=2, concat_axis=0, tiled=True)  14.9 us
    all_to_all x1, starting transfers between devices, shards(): lax.all_to_all(hidden, 'kv', split_axis=0, concat_axis=2, tiled=True)  7.42 us
    select_n x1, other arithmetic, shards(): state = jnp.where(live, moved, state)  7.13 us
    unnamed x17, local copies, waits for them, and re-layouts  5.27 us
    convert_element_type x2, local copies, waits for them, and re-layouts, shards(): whole_vals = arrived.astype(jnp.float32)  3.03 us
    dot_general x1, matrix products, shards(): jnp.dot(normed, w_query, preferred_element_type=jnp.float32)  2.17 us
  transfers between devices with their start and end apart: 1, of which 0 were waited for; matrix products, arithmetic and copies ran while one was open for 13% of the time, Pallas kernels for 0%

commit v1 on v0

--- a/solution.py
+++ b/solution.py
@@ -23,7 +23,10 @@
     prev_input,
     accepted,
 ):
-    arrived = lax.all_to_all(hidden, "kv", split_axis=0, concat_axis=2, tiled=True)
+    arrived = jnp.concatenate(
+        lax.all_to_all(jnp.stack(jnp.split(hidden, lax.axis_size("kv"), axis=0)), "kv", 0, 0),
+        axis=2,
+    )
     whole_vals = arrived.astype(jnp.float32)
     row_sums = jnp.sum(whole_vals * whole_vals, axis=2)
     normed = (whole_vals * lax.rsqrt(row_sums / D + 1e-06)[..., None] * norm_gain).astype(

time: 96.9 us -> 108 us (1.11)
  local copies, waits for them, and re-layouts: 17 us -> 28.1 us
    unnamed x17 -> x23, local copies, waits for them, and re-layouts: 5.27 us -> 15 us
    another operation x0 -> x1, local copies, waits for them, and re-layouts: none -> 1.38 us  [shards(): jnp.stack(jnp.split(hidden, lax.axis_size('kv'), axis=0))]
  transfers between devices with their start and end apart: 1 -> 1, of which waited for: 0 -> 0; matrix products, arithmetic and copies ran while one was open for 13% -> 12% of each run, Pallas kernels for 0% -> 0%
where the time goes in v1:
time: 108 us; the launch traced here: 107 us
  blocking collectives  31.5 us (29%)
  local copies, waits for them, and re-layouts  28.1 us (26%)
  matrix products  27.6 us (26%)
  other arithmetic  11.5 us (11%)
  starting transfers between devices  7.28 us (7%)
    dot_general x4, matrix products, shards(): jnp.einsum('bhk,bhkv->bhv', query[:, step], state, precision=lax.Precisio...  20.3 us
    psum x1, blocking collectives, shards(): finished = lax.psum(partial_value, 'tp').astype(jnp.bfloat16)  16.6 us
    unnamed x23, local copies, waits for them, and re-layouts  15 us
    all_to_all x1, blocking collectives, shards(): lax.all_to_all(finished, 'kv', split_axis=2, concat_axis=0, tiled=True)  14.9 us
    all_to_all x1, starting transfers between devices, shards(): lax.all_to_all(jnp.stack(jnp.split(hidden, lax.axis_size('kv'), axis=0)),...  7.28 us
    select_n x1, other arithmetic, shards(): state = jnp.where(live, moved, state)  7.13 us
    convert_element_type x2, local copies, waits for them, and re-layouts, shards(): whole_vals = arrived.astype(jnp.float32)  3.01 us
    dot_general x1, matrix products, shards(): jnp.dot(normed, w_query, preferred_element_type=jnp.float32)  2.17 us
  transfers between devices with their start and end apart: 1, of which 0 were waited for; matrix products, arithmetic and copies ran while one was open for 12% of the time, Pallas kernels for 0%

profile of v1, /device:TPU:0, one launch (start us, length us, event | category | flops | bytes accessed | tf_op | source)
XLA Modules:
  0.0 107.0 jit_solution(11793273186378179741)
XLA Ops:
  0.6 1.5 %bitcast_dynamic-update-slice_fusion.7 = bf16[8,16,4,256]{3,2,1,0:T(4,128)(2,1)} fusion(bf16[128,4,256]{2,1,0:T(4,128)(2,1)} %param.13), kind=kLoop, calls=%fused_computation.63 | loop fusion | bytes 65536
  2.1 1.4 %bitcast_dynamic-update-slice_fusion.6 = bf16[8,16,4,256]{3,2,1,0:T(4,128)(2,1)} fusion(bf16[8,16,4,256]{3,2,1,0:T(4,128)(2,1)} %bitcast_dynamic-update-slice_fusion.7, bf16[128,4,256]{2,1,0:T(4,128)(2,1)} %param.13), kind=kLoop, calls=%fused_computation.62 | loop fusion | bytes 65536
  3.5 1.4 %bitcast_dynamic-update-slice_fusion.5 = bf16[8,16,4,256]{3,2,1,0:T(4,128)(2,1)} fusion(bf16[8,16,4,256]{3,2,1,0:T(4,128)(2,1)} %bitcast_dynamic-update-slice_fusion.6, bf16[128,4,256]{2,1,0:T(4,128)(2,1)} %param.13), kind=kLoop, calls=%fused_computation.61 | loop fusion | bytes 65536
  4.9 1.4 %bitcast_dynamic-update-slice_fusion.4 = bf16[8,16,4,256]{3,2,1,0:T(4,128)(2,1)} fusion(bf16[8,16,4,256]{3,2,1,0:T(4,128)(2,1)} %bitcast_dynamic-update-slice_fusion.5, bf16[128,4,256]{2,1,0:T(4,128)(2,1)} %param.13), kind=kLoop, calls=%fused_computation.60 | loop fusion | bytes 65536
  6.3 1.4 %bitcast_dynamic-update-slice_fusion.3 = bf16[8,16,4,256]{3,2,1,0:T(4,128)(2,1)} fusion(bf16[8,16,4,256]{3,2,1,0:T(4,128)(2,1)} %bitcast_dynamic-update-slice_fusion.4, bf16[128,4,256]{2,1,0:T(4,128)(2,1)} %param.13), kind=kLoop, calls=%fused_computation.59 | loop fusion | bytes 65536
  7.7 1.4 %bitcast_dynamic-update-slice_fusion.2 = bf16[8,16,4,256]{3,2,1,0:T(4,128)(2,1)} fusion(bf16[8,16,4,256]{3,2,1,0:T(4,128)(2,1)} %bitcast_dynamic-update-slice_fusion.3, bf16[128,4,256]{2,1,0:T(4,128)(2,1)} %param.13), kind=kLoop, calls=%fused_computation.58 | loop fusion | bytes 65536
  9.0 1.4 %bitcast_dynamic-update-slice_fusion.1 = bf16[8,16,4,256]{3,2,1,0:T(4,128)(2,1)} fusion(bf16[8,16,4,256]{3,2,1,0:T(4,128)(2,1)} %bitcast_dynamic-update-slice_fusion.2, bf16[128,4,256]{2,1,0:T(4,128)(2,1)} %param.13), kind=kLoop, calls=%fused_computation.57 | loop fusion | bytes 65536
  10.4 1.4 %bitcast_dynamic-update-slice_fusion = bf16[8,16,4,256]{3,2,1,0:T(4,128)(2,1)} fusion(bf16[8,16,4,256]{3,2,1,0:T(4,128)(2,1)} %bitcast_dynamic-update-slice_fusion.1, bf16[128,4,256]{2,1,0:T(4,128)(2,1)} %param.13), kind=kLoop, calls=%fused_computation.56 | loop fusion | bytes 65536 | tf_op jit(solution)/shard_map/stack | solution.py:27
  11.8 7.3 %all-to-all-start = ((bf16[8,16,4,256]{3,2,1,0:T(4,128)(2,1)}), bf16[8,16,4,256]{3,2,1,0:T(4,128)(2,1)S(1)}, u32[]{:S(2)}, u32[]{:S(2)}) async-start(bf16[8,16,4,256]{3,2,1,0:T(4,128)(2,1)} %bitcast_dynamic-update-slice_fusion), calls=%async_computation | async-start | bytes 524288 | tf_op jit(solution)/shard_map/all_to_all | solution.py:27
  20.3 0.8 multiply_add_fusion.9
  21.2 1.2 %broadcast_bitcast_fusion = f32[256]{0:T(256)} fusion(f32[128]{0:T(128)} %param.21), kind=kLoop, calls=%fused_computation.92 | loop fusion | bytes 1536 | tf_op jit(solution)/shard_map/mul | solution.py:69
  22.5 1.2 %broadcast_compare_fusion.3 = (pred[16]{0:T(512)(128)(4,1)}, pred[16]{0:T(512)(128)(4,1)}, pred[16]{0:T(512)(128)(4,1)}, pred[16]{0:T(512)(128)(4,1)}) fusion(s32[16]{0:T(128)} %param.25), kind=kLoop, calls=%fused_computation.98 | loop fusion | flops 64 | bytes 128 | tf_op jit(solution)/shard_map/gt | solution.py:51
  23.7 0.8 reshape.127
  25.1 7.1 %add_select_fusion = f32[16,2,128,128]{3,2,1,0:T(8,128)S(1)} fusion(f32[16,2,128,128]{3,2,1,0:T(8,128)} %param.22, f32[16,2,128]{2,1,0:T(2,128)} %get-tuple-element.29, f32[16,2,128]{2,1,0:T(2,128)S(1)} %get-tuple-element.25, f32[16,2,128]{2,1,0:T(2,128)} %get-tuple-element.27, f32[16,2,128]{2,1,0:T(2,128)S(1)} %get-tuple-element.24, ...), kind=kLoop, calls=%fused_computation.7 | loop fusion | flops 8388608 | bytes 4390976 | tf_op jit(solution)/shard_map/jit(_where)/select_n | solution.py:56
  32.7 1.1 %copy.37 = f32[16,4,8,256]{3,2,0,1:T(8,128)} copy(f32[16,4,8,256]{3,1,0,2:T(4,128)S(1)} %convert_bitcast_fusion) | data formatting | bytes 1048576 | tf_op jit(solution)/shard_map/convert_element_type | solution.py:30
  33.8 1.9 %reshape.125 = f32[16,4,2048]{2,0,1:T(8,128)} reshape(f32[16,4,8,256]{3,2,0,1:T(8,128)} %copy.37) | data formatting | bytes 1048576 | tf_op jit(solution)/shard_map/convert_element_type | solution.py:30
  35.7 1.2 %multiply_convert_fusion = bf16[16,4,2048]{2,0,1:T(8,128)(2,1)S(1)} fusion(f32[16,4,2048]{2,0,1:T(8,128)} %reshape.125, f32[2048]{0:T(1024)S(1)} %copy-done.5, f32[16,4]{0,1:T(4,128)S(1)} %add_rsqrt_fusion.1), kind=kLoop, calls=%fused_computation.46 | loop fusion | flops 393216 | bytes 794880 | tf_op jit(solution)/shard_map/convert_element_type | solution.py:32
  36.9 1.5 %fusion.14 = f32[16,4,256]{2,0,1:T(8,128)S(1)} fusion(bf16[16,4,2048]{2,0,1:T(8,128)(2,1)S(1)} %multiply_convert_fusion, bf16[2048,256]{1,0:T(8,128)(2,1)} %param.16, f32[256]{0:T(256)S(1)} %copy-done.4, f32[256]{0:T(256)S(1)} %copy-done.2), kind=kOutput, calls=%fused_computation.21 | convolution fusion | flops 67223552 | bytes 1378304 | tf_op jit(solution)/shard_map/dot_general | solution.py:36
  38.5 1.5 %fusion.7 = f32[16,4,256]{2,0,1:T(8,128)S(1)} fusion(bf16[16,4,2048]{2,0,1:T(8,128)(2,1)S(1)} %multiply_convert_fusion, bf16[2048,256]{1,0:T(8,128)(2,1)} %param.17), kind=kOutput, calls=%fused_computation.13 | convolution fusion | flops 67141632 | bytes 1376256 | tf_op jit(solution)/shard_map/dot_general | solution.py:37
  40.7 2.2 %divide_multiply_fusion = f32[16,4,256]{2,0,1:T(8,128)} fusion(bf16[16,4,2048]{2,0,1:T(8,128)(2,1)S(1)} %multiply_convert_fusion, bf16[2048,256]{1,0:T(8,128)(2,1)} %param.15), kind=kOutput, calls=%fused_computation.55 | convolution fusion | flops 67207168 | bytes 1376256 | tf_op jit(solution)/shard_map/dot_general | solution.py:35
  42.8 0.9 reshape.118
  44.6 2.8 %fusion.4 = f32[16,2,1,128]{3,2,1,0:T(1,128)S(1)} fusion(f32[16,2,128,1]{2,3,1,0:T(1,128)S(1)} %bitcast.158, f32[16,2,128,128]{3,2,1,0:T(8,128)S(1)} %add_select_fusion, f32[16,2,128]{2,1,0:T(2,128)S(1)} %get-tuple-element.14, f32[16,2,128]{2,1,0:T(2,128)S(1)} %get-tuple-element.10, f32[16,2,128]{2,1,0:T(2,128)S(1)} %get-tuple-element.37), kind=kOutput, calls=%fused_computation.8 | convolution fusion | flops 7864320 | bytes 2179072 | tf_op jit(solution)/shard_map/bhk,bhkv->bhv/dot_general | solution.py:65
  47.4 4.3 %fusion.36 = f32[16,2,1,128]{3,2,1,0:T(1,128)S(1)} fusion(f32[16,2,128,1]{2,3,1,0:T(1,128)S(1)} %bitcast.167, f32[16,2,128,128]{3,2,1,0:T(8,128)S(1)} %add_select_fusion, f32[16,2,128]{2,1,0:T(2,128)S(1)} %get-tuple-element.17, f32[16,2,128]{2,1,0:T(2,128)S(1)} %get-tuple-element.13, f32[16,2,128]{2,1,0:T(2,128)S(1)} %get-tuple-element.34, ...), kind=kOutput, calls=%fused_computation.47 | convolution fusion | flops 9437184 | bytes 2228224 | tf_op jit(solution)/shard_map/bhk,bhkv->bhv/dot_general | solution.py:65
  51.6 6.1 %fusion.5 = f32[16,2,1,128]{3,2,1,0:T(1,128)S(1)} fusion(f32[16,2,128,1]{2,3,1,0:T(1,128)S(1)} %bitcast.166, f32[16,2,128]{2,1,0:T(2,128)S(1)} %get-tuple-element.16, f32[16,2,128]{2,1,0:T(2,128)S(1)} %get-tuple-element.12, f32[16,2,128]{2,1,0:T(2,128)S(1)} %get-tuple-element.35, f32[16,2,128,128]{3,2,1,0:T(8,128)S(1)} %add_select_fusion, ...), kind=kOutput, calls=%fused_computation.9 | convolution fusion | flops 11010048 | bytes 2277376 | tf_op jit(solution)/shard_map/bhk,bhkv->bhv/dot_general | solution.py:65
  57.7 7.2 %fusion = f32[16,2,1,128]{3,2,1,0:T(1,128)S(1)} fusion(f32[16,2,128,1]{2,3,1,0:T(1,128)S(1)} %bitcast.165, f32[16,2,128]{2,1,0:T(2,128)S(1)} %get-tuple-element.15, f32[16,2,128]{2,1,0:T(2,128)S(1)} %get-tuple-element.11, f32[16,2,128]{2,1,0:T(2,128)S(1)} %get-tuple-element.36, f32[16,2,128]{2,1,0:T(2,128)S(1)} %get-tuple-element.16, ...), kind=kOutput, calls=%fused_computation | convolution fusion | flops 12582912 | bytes 2326528 | tf_op jit(solution)/shard_map/bhk,bhkv->bhv/dot_general | solution.py:65
  65.4 2.0 %fusion.16 = f32[16,4,2048]{2,0,1:T(8,128)S(1)} fusion(bf16[1024,2048]{1,0:T(8,128)(2,1)} %param.19, s32[]{:T(128)S(6)} %select_n.20, f32[16,4,256]{2,0,1:T(8,128)S(1)} %mul.343, f32[16,1,256]{2,0,1:T(8,128)S(1)} %stack.64, f32[16,1,256]{2,0,1:T(8,128)S(1)} %stack.63, f32[16,1,256]{2,0,1:T(8,128)S(1)} %stack.62, f32[16,1,256]{2,0,1:T(8,128)S(1)} %stack.61, ...), kind=kOutput, calls=%fused_computation.24 | convolution fusion | flops 134430720 | bytes 3015684 | tf_op jit(solution)/shard_map/dot_general | solution.py:75
  67.5 16.6 %all-reduce.1 = bf16[16,4,2048]{2,0,1:T(8,128)(2,1)S(1)} all-reduce(f32[16,4,2048]{2,0,1:T(8,128)S(1)} %fusion.16), channel_id=1, replica_groups=mesh['kv'=8,'tp'=4] {'tp'}, use_global_device_ids=true, to_apply=%region_2.3 | all-reduce | flops 131072 | bytes 786432 | tf_op jit(solution)/shard_map/psum | solution.py:76
  84.1 1.4 %copy.44 = bf16[16,4,2048]{0,1,2:T(4,128)(2,1)S(1)} copy(bf16[16,4,2048]{2,0,1:T(8,128)(2,1)S(1)} %all-reduce.1) | data formatting | bytes 524288 | tf_op jit(solution)/shard_map/convert_element_type | solution.py:76
  85.5 2.2 %reshape.144 = bf16[8,2,8192]{2,1,0:T(2,128)(2,1)S(1)} reshape(bf16[2048,4,16]{2,1,0:T(4,128)(2,1)S(1)} %bitcast.153) | data formatting | bytes 524288
  87.7 14.9 %all_to_all.23 = bf16[8,2,8192]{2,1,0:T(2,128)(2,1)} all-to-all(bf16[8,2,8192]{2,1,0:T(2,128)(2,1)S(1)} %reshape.144), channel_id=1, replica_groups=mesh['kv'=8,'tp'=4] {'kv'}, dimensions={0} | all-to-all | bytes 524288 | tf_op jit(solution)/shard_map/all_to_all | solution.py:77
  102.5 2.4 %reshape.145 = bf16[2048,4,16]{2,1,0:T(4,128)(2,1)S(1)} reshape(bf16[8,2,8192]{2,1,0:T(2,128)(2,1)} %all_to_all.23) | data formatting | bytes 524288
  104.9 2.0 %copy.45 = bf16[8,16,4,256]{3,2,1,0:T(4,128)(2,1)} copy(bf16[8,16,4,256]{1,2,3,0:T(4,128)(2,1)S(1)} %bitcast.154) | data formatting | bytes 524288 | tf_op jit(solution)/shard_map/all_to_all | solution.py:77
  (37 shorter events, 4.3 us)
Async XLA Ops:
  0.6 64.8 %copy-start = (bf16[2048,256]{1,0:T(8,128)(2,1)S(1)}, bf16[2048,256]{1,0:T(8,128)(2,1)}, u32[]{:S(2)}) copy-start(bf16[2048,256]{1,0:T(8,128)(2,1)} %param.18) | copy-start | bytes 3145732
  11.8 20.5 %all-to-all-start = ((bf16[8,16,4,256]{3,2,1,0:T(4,128)(2,1)}), bf16[8,16,4,256]{3,2,1,0:T(4,128)(2,1)S(1)}, u32[]{:S(2)}, u32[]{:S(2)}) async-start(bf16[8,16,4,256]{3,2,1,0:T(4,128)(2,1)} %bitcast_dynamic-update-slice_fusion), calls=%async_computation | async-start | bytes 524288 | tf_op jit(solution)/shard_map/all_to_all | solution.py:27
  19.8 0.6 copy-start.3
  32.3 25.5 %copy-start.1 = (f32[16,2,128,128]{3,2,1,0:T(8,128)}, f32[16,2,128,128]{3,2,1,0:T(8,128)S(1)}, u32[]{:S(2)}) copy-start(f32[16,2,128,128]{3,2,1,0:T(8,128)S(1)} %add_select_fusion) | copy-start | bytes 6291460
  32.3 3.5 %copy-start.5 = (f32[2048]{0:T(1024)S(1)}, f32[2048]{0:T(1024)}, u32[]{:S(2)}) copy-start(f32[2048]{0:T(1024)} %param.14) | copy-start | bytes 24580
  32.3 4.6 %copy-start.2 = (f32[256]{0:T(256)S(1)}, f32[256]{0:T(256)}, u32[]{:S(2)}) copy-start(f32[256]{0:T(256)} %param.20) | copy-start | bytes 3076
  32.3 4.6 %copy-start.4 = (f32[256]{0:T(256)S(1)}, f32[256]{0:T(256)}, u32[]{:S(2)}) copy-start(f32[256]{0:T(256)} %copy-done.3) | copy-start | bytes 3076
  57.7 7.7 %copy-start.6 = (f32[256]{0:T(256)S(1)}, f32[256]{0:T(256)}, u32[]{:S(2)}) copy-start(f32[256]{0:T(256)} %broadcast_bitcast_fusion) | copy-start | bytes 3076
